TPU v7x, 32 devices: a whole 2x2x4 slice. The times are simulated.
32 devices in a mesh: sp: 8 (over z, x), dp: 4 (over y, core).
Axes of the slice: x: 2, y: 2, z: 4, core: 2. Of those that a mesh axis runs over, the one named last changes fastest.
Arguments:
- queries: bfloat16 [4, 1024, 2048], P('dp', 'sp'), may hold values from -6 to 6
- forget_pre: bfloat16 [4, 1024, 2048], P('dp', 'sp'), may hold values from -5.5 to 5.5
- values: bfloat16 [4, 1024, 2048], P('dp', 'sp'), may hold values from -6 to 6
- out_gate: bfloat16 [4, 1024, 2048], P('dp', 'sp'), may hold values from -6 to 6
- lower_bound: float32 [2048], P('sp'), may hold values from 0.9 to 1, as said below
- head_gain: float32 [128], replicated, may hold values from 0.1 to 1.9
- residual: bfloat16 [4, 1024, 4096], P('dp', 'sp'), may hold values from -6 to 6
- out_weight: bfloat16 [2048, 4096], P(None, 'dp'), may hold values from -0.125 to 0.125
- ffn_gain: float32 [4096], replicated, may hold values from 0.1 to 1.9
- routing: int32 [4, 1024, 4], P('dp', 'sp'), may hold values from 0 to 31, all different within a row; in each aligned block of 128 rows (0 to 127, 128 to 255, ..., all dimensions but the last counted through in order) at most 20 rows name the same one
- route_weight: float32 [4, 1024, 4], P('dp', 'sp'), may hold values from 0.1 to 1
- expert_gate: bfloat16 [32, 4096, 512], P(('sp', 'dp')), may hold values from -0.09375 to 0.09375
- expert_up: bfloat16 [32, 4096, 512], P(('sp', 'dp')), may hold values from -0.09375 to 0.09375
- expert_down: bfloat16 [32, 512, 4096], P(('sp', 'dp')), may hold values from -0.25 to 0.25
Outputs:
- layer_out: bfloat16 [4, 1024, 4096], P('dp', 'sp')
Inputs may be any that keep to these rules, and one draw needn't show every extreme that they name: `routing`: within the rows of one device no expert is named more than 20 times, and in some devices one is named exactly 20 times; the 4 experts of a row differ. `lower_bound`: every entry is below 1.
All inputs are finite; a program needn't handle non-finite values.
Results may differ from a plain program's by a relative error of at most 0.0073.
Values may be sent and summed in bfloat16 or wider, within the bound.
A program may use at most 128 MiB of HBM per device.

v0:
```python
import functools

import jax
import jax.numpy as jnp
from jax import lax
from jax.experimental import pallas as pl
from jax.experimental.pallas import tpu as pltpu
from jax.sharding import PartitionSpec as P

MESH = pl.DeviceIdType.MESH
VMEM_WHOLE = pl.BlockSpec(memory_space=pltpu.VMEM)

CHUNK = 512
GATED_PARTS = 4


NORM_EPS = 1e-06


def wait_bytes(ref, sem):
    pltpu.make_async_copy(ref, ref, sem).wait()


def place(nz, nx, ndp):
    sp, dp = lax.axis_index("sp"), lax.axis_index("dp")
    z = lax.div(sp, nx)
    me = lax.rem(sp, nx) * ndp + dp
    above, below = {"sp": sp + nx, "dp": dp}, {"sp": sp - nx, "dp": dp}

    def member(p):
        return {"sp": z * nx + lax.div(p, ndp), "dp": lax.rem(p, ndp)}

    return z, me, above, below, member


def greet(nz, peers, z, me, above, below, member):
    barrier = pltpu.get_barrier_semaphore()

    @pl.when(z > 0)
    def _():
        pl.semaphore_signal(barrier, inc=1, device_id=below, device_id_type=MESH)

    @pl.when(z < nz - 1)
    def _():
        pl.semaphore_signal(barrier, inc=1, device_id=above, device_id_type=MESH)

    def one(k, carry):
        pl.semaphore_signal(
            barrier, inc=1, device_id=member(lax.rem(me + k, peers)), device_id_type=MESH
        )
        return carry

    lax.fori_loop(1, peers, one, 0)
    count = peers - 1 + jnp.where(z > 0, 1, 0) + jnp.where(z < nz - 1, 1, 0)
    pl.semaphore_wait(barrier, count)


def dispatch_kernel(
    nz,
    nx,
    ndp,
    width,
    x_ref,
    pick_ref,
    gate_ref,
    lift_ref,
    act_ref,
    gath,
    slots,
    got,
    gate_sum,
    lift_sum,
    up_send,
    dn_send,
    line_recv,
    pl_send,
    pl_recv,
):
    peers = nx * ndp
    z, me, above, below, member = place(nz, nx, ndp)
    tok, model = x_ref.shape
    chunks = model // width
    per = act_ref.shape[0] // peers
    greet(nz, peers, z, me, above, below, member)

    def block(b):
        return pl.ds(pl.multiple_of(b * tok, tok), tok)

    def share(p):
        return pl.ds(pl.multiple_of(p * per, per), per)

    def pass_on(src, b, c, cols, sem, device):
        pltpu.make_async_remote_copy(
            src_ref=src,
            dst_ref=gath.at[block(b), cols],
            send_sem=sem,
            recv_sem=line_recv.at[b, c],
            device_id=device,
            device_id_type=MESH,
        ).start()

    gath[block(z), :] = x_ref[...]
    gate_sum[...] = jnp.zeros_like(gate_sum)
    lift_sum[...] = jnp.zeros_like(lift_sum)

    def tick(t, carry):
        for s in range(nz):
            c = t - s
            cols = pl.ds(pl.multiple_of(c * width, width), width)
            valid = (c >= 0) & (c < chunks)
            if s == 0:

                @pl.when(valid & (z < nz - 1))
                def _():
                    pass_on(x_ref.at[:, cols], z, c, cols, up_send.at[0], above)

                @pl.when(valid & (z > 0))
                def _():
                    pass_on(x_ref.at[:, cols], z, c, cols, dn_send.at[0], below)

                continue

            @pl.when(valid & (z - s >= 0))
            def _():
                b = z - s
                here = gath.at[block(b), cols]
                wait_bytes(here, line_recv.at[b, c])

                @pl.when(z < nz - 1)
                def _():
                    pass_on(here, b, c, cols, up_send.at[s], above)

            @pl.when(valid & (z + s < nz))
            def _():
                b = z + s
                here = gath.at[block(b), cols]
                wait_bytes(here, line_recv.at[b, c])

                @pl.when(z > 0)
                def _():
                    pass_on(here, b, c, cols, dn_send.at[s], below)

        c = t - (nz - 1)

        @pl.when((c >= 0) & (c < chunks))
        def _():
            cols = pl.ds(pl.multiple_of(c * width, width), width)
            slots[:, cols] = jnp.dot(
                pick_ref[...], gath[:, cols], preferred_element_type=jnp.float32
            ).astype(jnp.bfloat16)
            got[share(me), cols] = slots[share(me), cols]

            def send(k, inner):
                p = lax.rem(me + k, peers)
                pltpu.make_async_remote_copy(
                    src_ref=slots.at[share(p), cols],
                    dst_ref=got.at[share(me), cols],
                    send_sem=pl_send.at[k],
                    recv_sem=pl_recv.at[k, c],
                    device_id=member(p),
                    device_id_type=MESH,
                ).start()
                return inner

            lax.fori_loop(1, peers, send, 0)

        late = t - nz

        @pl.when(late >= 0)
        def _():
            cols = pl.ds(pl.multiple_of(late * width, width), width)

            def arrive(k, inner):
                p = lax.rem(me + peers - k, peers)
                wait_bytes(got.at[share(p), cols], pl_recv.at[k, late])
                return inner

            lax.fori_loop(1, peers, arrive, 0)
            rows = got[:, cols]
            gate_sum[...] += jnp.dot(rows, gate_ref[cols, :], preferred_element_type=jnp.float32)
            lift_sum[...] += jnp.dot(rows, lift_ref[cols, :], preferred_element_type=jnp.float32)

        return carry

    lax.fori_loop(0, chunks + nz, tick, 0)
    gate = gate_sum[...]
    act_ref[...] = (gate / (1.0 + jnp.exp(-gate)) * lift_sum[...]).astype(jnp.bfloat16)

    for s in range(nz - 1):

        @pl.when((z - s >= 0) & (z < nz - 1))
        def _():
            wait_bytes(x_ref, up_send.at[s])

        @pl.when((z + s < nz) & (z > 0))
        def _():
            wait_bytes(x_ref, dn_send.at[s])

    def finish(k, carry):
        wait_bytes(slots.at[share(lax.rem(me + k, peers)), :], pl_send.at[k])
        return carry

    lax.fori_loop(1, peers, finish, 0)


def return_kernel(
    nz,
    nx,
    ndp,
    width,
    act_ref,
    down_ref,
    high_ref,
    low_ref,
    h_ref,
    out_ref,
    r_ref,
    ret,
    part,
    up_out,
    up_in,
    dn_out,
    dn_in,
    pl_send,
    pl_recv,
    up_send,
    dn_send,
    up_recv,
    dn_recv,
):
    peers = nx * ndp
    z, me, above, below, member = place(nz, nx, ndp)
    tok, model = h_ref.shape
    chunks = model // width
    per = r_ref.shape[0] // peers
    greet(nz, peers, z, me, above, below, member)

    def block(b):
        return pl.ds(pl.multiple_of(b * tok, tok), tok)

    def share(p):
        return pl.ds(pl.multiple_of(p * per, per), per)

    def columns(c):
        return pl.ds(pl.multiple_of(c * width, width), width)

    def send_chunk(c, carry):
        r_ref[:, columns(c)] = jnp.dot(
            act_ref[...], down_ref[:, columns(c)], preferred_element_type=jnp.float32
        ).astype(jnp.bfloat16)

        def send(k, inner):
            p = lax.rem(me + k, peers)
            pltpu.make_async_remote_copy(
                src_ref=r_ref.at[share(p), columns(c)],
                dst_ref=ret.at[share(me), columns(c)],
                send_sem=pl_send.at[k],
                recv_sem=pl_recv.at[k, c],
                device_id=member(p),
                device_id_type=MESH,
            ).start()
            return inner

        return lax.fori_loop(1, peers, send, carry)

    lax.fori_loop(0, chunks, send_chunk, 0)
    ret[share(me), :] = r_ref[share(me), :]

    def line(c, first, sends, takes, inbox, outbox, send_sem, recv_sem, device):
        cols = columns(c)
        for d in range(nz):
            rows = pl.ds(d * tok, tok)

            @pl.when(jnp.logical_not(first) & takes(d))
            def _():
                wait_bytes(inbox.at[rows, cols], recv_sem.at[d, c])

            @pl.when(sends(d))
            def _():
                @pl.when(first)
                def _():
                    outbox[rows, cols] = part[rows, cols].astype(jnp.bfloat16)

                @pl.when(jnp.logical_not(first))
                def _():
                    outbox[rows, cols] = (
                        part[rows, cols] + inbox[rows, cols].astype(jnp.float32)
                    ).astype(jnp.bfloat16)

                pltpu.make_async_remote_copy(
                    src_ref=outbox.at[rows, cols],
                    dst_ref=inbox.at[rows, cols],
                    send_sem=send_sem.at[d],
                    recv_sem=recv_sem.at[d, c],
                    device_id=device,
                    device_id_type=MESH,
                ).start()

    def tick(t, carry):
        @pl.when(t < chunks)
        def _():
            cols = columns(t)

            def arrive(k, inner):
                p = lax.rem(me + peers - k, peers)
                wait_bytes(ret.at[share(p), cols], pl_recv.at[k, t])
                return inner

            lax.fori_loop(1, peers, arrive, 0)
            rows = ret[:, cols]
            part[:, cols] = jnp.dot(
                high_ref[...], rows, preferred_element_type=jnp.float32
            ) + jnp.dot(low_ref[...], rows, preferred_element_type=jnp.float32)

        cu = t - z

        @pl.when((cu >= 0) & (cu < chunks))
        def _():
            line(
                cu, z == 0, lambda d: d > z, lambda d: d >= z, up_in, up_out, up_send, up_recv, above
            )

        cd = t - (nz - 1 - z)

        @pl.when((cd >= 0) & (cd < chunks))
        def _():
            line(
                cd, z == nz - 1, lambda d: d < z, lambda d: d <= z, dn_in, dn_out, dn_send, dn_recv, below
            )

        return carry

    lax.fori_loop(0, chunks + nz - 1, tick, 0)

    own = block(z)

    @pl.when(z > 0)
    def _():
        part[own, :] = part[own, :] + up_in[own, :].astype(jnp.float32)

    @pl.when(z < nz - 1)
    def _():
        part[own, :] = part[own, :] + dn_in[own, :].astype(jnp.float32)

    out_ref[...] = (h_ref[...].astype(jnp.float32) + part[own, :]).astype(jnp.bfloat16)

    for d in range(nz):

        @pl.when(d > z)
        def _():
            wait_bytes(up_out.at[pl.ds(d * tok, tok), :], up_send.at[d])

        @pl.when(d < z)
        def _():
            wait_bytes(dn_out.at[pl.ds(d * tok, tok), :], dn_send.at[d])

    def finish(k, carry):
        wait_bytes(r_ref.at[share(lax.rem(me + k, peers)), :], pl_send.at[k])
        return carry

    lax.fori_loop(1, peers, finish, 0)


def routing_tables(packed, nz, nx, ndp, cap, per):
    tok, top = packed.shape[1], packed.shape[2] // 2
    peers = nx * ndp
    sp = lax.axis_index("sp")
    z, x = sp // nx, sp % nx
    packed = lax.dynamic_index_in_dim(packed.reshape(nz, nx, tok, 2 * top), x, 1, keepdims=False)
    chosen = packed[..., :top].astype(jnp.int32)
    experts = z * peers + jnp.arange(peers, dtype=jnp.int32)
    same = chosen[:, :, :, None] == experts
    named = jnp.any(same, axis=2)
    weight = jnp.sum(jnp.where(same, packed[..., top:, None], 0.0), axis=2)
    earlier = jnp.tril(jnp.ones((tok, tok), jnp.bfloat16), -1)
    rank = jnp.einsum(
        "ts,bsp->btp", earlier, named.astype(jnp.bfloat16), preferred_element_type=jnp.float32
    ).astype(jnp.int32)
    slot = jnp.arange(nz, dtype=jnp.int32)[:, None, None] * cap + rank
    slot = jnp.where(named, slot, per)
    slot_ids = jnp.arange(per, dtype=jnp.int32)
    pick = slot.transpose(2, 0, 1)[:, None, :, :] == slot_ids[None, :, None, None]
    pick = pick.astype(jnp.bfloat16).reshape(peers * per, nz * tok)
    mixed = jnp.where(slot[..., None] == slot_ids, weight[..., None], 0.0)
    mixed = mixed.reshape(nz * tok, peers * per)
    high = lax.reduce_precision(mixed, 8, 7)
    return pick, high.astype(jnp.bfloat16), (mixed - high).astype(jnp.bfloat16)


def dispatch(moe_in, pick, w_gate, w_up, nz, nx, ndp, width):
    tok, model = moe_in.shape
    inner = w_gate.shape[1]
    peers = nx * ndp
    total = pick.shape[0]
    chunks = model // width
    bf16 = jnp.bfloat16
    return pl.pallas_call(
        functools.partial(dispatch_kernel, nz, nx, ndp, width),
        out_shape=jax.ShapeDtypeStruct((total, inner), bf16),
        in_specs=[VMEM_WHOLE] * 4,
        out_specs=VMEM_WHOLE,
        scratch_shapes=[
            pltpu.VMEM((nz * tok, model), bf16),
            pltpu.VMEM((total, model), bf16),
            pltpu.VMEM((total, model), bf16),
            pltpu.VMEM((total, inner), jnp.float32),
            pltpu.VMEM((total, inner), jnp.float32),
            pltpu.SemaphoreType.DMA((nz,)),
            pltpu.SemaphoreType.DMA((nz,)),
            pltpu.SemaphoreType.DMA((nz, chunks)),
            pltpu.SemaphoreType.DMA((peers,)),
            pltpu.SemaphoreType.DMA((peers, chunks)),
        ],
        compiler_params=pltpu.CompilerParams(
            collective_id=1, has_side_effects=True, vmem_limit_bytes=60 * 1024 * 1024
        ),
    )(moe_in, pick, w_gate, w_up)


def combine(act, w_down, high, low, hidden, nz, nx, ndp, width):
    tok, model = hidden.shape
    peers = nx * ndp
    total = act.shape[0]
    chunks = model // width
    bf16 = jnp.bfloat16
    return pl.pallas_call(
        functools.partial(return_kernel, nz, nx, ndp, width),
        out_shape=jax.ShapeDtypeStruct((tok, model), bf16),
        in_specs=[VMEM_WHOLE] * 5,
        out_specs=VMEM_WHOLE,
        scratch_shapes=[
            pltpu.VMEM((total, model), bf16),
            pltpu.VMEM((total, model), bf16),
            pltpu.VMEM((nz * tok, model), jnp.float32),
            pltpu.VMEM((nz * tok, model), bf16),
            pltpu.VMEM((nz * tok, model), bf16),
            pltpu.VMEM((nz * tok, model), bf16),
            pltpu.VMEM((nz * tok, model), bf16),
            pltpu.SemaphoreType.DMA((peers,)),
            pltpu.SemaphoreType.DMA((peers, chunks)),
            pltpu.SemaphoreType.DMA((nz,)),
            pltpu.SemaphoreType.DMA((nz,)),
            pltpu.SemaphoreType.DMA((nz, chunks)),
            pltpu.SemaphoreType.DMA((nz, chunks)),
        ],
        compiler_params=pltpu.CompilerParams(
            collective_id=2, has_side_effects=True, vmem_limit_bytes=60 * 1024 * 1024
        ),
    )(act, w_down, high, low, hidden)


def mixer_kernel(
    n,
    q_ref,
    f_ref,
    v_ref,
    og_ref,
    bound_ref,
    gain_ref,
    out_ref,
    qs,
    ks,
    within,
    push,
    keep,
    push_in,
    keep_in,
    before_out,
    before_in,
    push_send,
    keep_send,
    push_recv,
    keep_recv,
    back_send,
    back_recv,
):
    me = lax.axis_index("sp")
    bf16, f32 = jnp.bfloat16, jnp.float32
    tok, _ = q_ref.shape
    heads, size, _ = push.shape
    own = heads // n
    barrier = pltpu.get_barrier_semaphore()

    def other(k):
        return lax.rem(me + k, n)

    def greet_one(k, carry):
        pl.semaphore_signal(barrier, inc=1, device_id={"sp": other(k)}, device_id_type=MESH)
        return carry

    lax.fori_loop(1, n, greet_one, 0)

    row = lax.broadcasted_iota(jnp.int32, (tok, tok), 0)
    col = lax.broadcasted_iota(jnp.int32, (tok, tok), 1)
    causal = row >= col
    lower = jnp.where(causal, 1.0, 0.0).astype(bf16)

    def columns(h):
        return pl.ds(pl.multiple_of(h * size, size), size)

    def group(j):
        return pl.ds(j * own, own)

    def prepare(h, carry):
        cols = columns(h)
        forget = f_ref[:, cols].astype(f32)
        leak = (1.0 - bound_ref[:, cols]) / (1.0 + jnp.exp(forget))
        log_keep = jnp.log1p(-leak)
        first = log_keep.astype(bf16)
        rest = log_keep - first.astype(f32)
        second = rest.astype(bf16)
        third = (rest - second.astype(f32)).astype(bf16)
        log_run = (
            jnp.dot(lower, first, preferred_element_type=f32)
            + jnp.dot(lower, second, preferred_element_type=f32)
            + jnp.dot(lower, third, preferred_element_type=f32)
        )
        last = log_run[tok - 1 : tok, :]
        ks[:, cols] = (leak * jnp.exp(-log_run)).astype(bf16)
        qs[:, cols] = (q_ref[:, cols].astype(f32) * jnp.exp(log_run)).astype(bf16)
        carry_key = (leak * jnp.exp(last - log_run)).astype(bf16)
        push[h] = lax.dot_general(
            v_ref[:, cols], carry_key, (((0,), (0,)), ((), ())), preferred_element_type=f32
        ).astype(bf16)
        keep[h] = jnp.broadcast_to(jnp.exp(last), (8, size))
        return carry

    lax.fori_loop(0, heads, prepare, 0)
    pl.semaphore_wait(barrier, n - 1)

    def send_push(k, carry):
        j = other(k)
        pltpu.make_async_remote_copy(
            src_ref=push.at[group(j)],
            dst_ref=push_in.at[group(me)],
            send_sem=push_send.at[k],
            recv_sem=push_recv.at[me],
            device_id={"sp": j},
            device_id_type=MESH,
        ).start()
        pltpu.make_async_remote_copy(
            src_ref=keep.at[group(j)],
            dst_ref=keep_in.at[group(me)],
            send_sem=keep_send.at[k],
            recv_sem=keep_recv.at[me],
            device_id={"sp": j},
            device_id_type=MESH,
        ).start()
        return carry

    lax.fori_loop(1, n, send_push, 0)
    push_in[group(me)] = push[group(me)]
    keep_in[group(me)] = keep[group(me)]

    def inside(h, carry):
        cols = columns(h)
        scores = lax.dot_general(
            qs[:, cols], ks[:, cols], (((1,), (1,)), ((), ())), preferred_element_type=f32
        )
        scores = jnp.where(causal, scores, 0.0).astype(bf16)
        within[:, cols] = jnp.dot(scores, v_ref[:, cols], preferred_element_type=f32)
        return carry

    lax.fori_loop(0, heads, inside, 0)

    def scan(b, states):
        @pl.when(b != me)
        def _():
            wait_bytes(push_in.at[group(b)], push_recv.at[b])
            wait_bytes(keep_in.at[group(b)], keep_recv.at[b])

        for i in range(own):
            before_out[b * own + i] = states[i].astype(bf16)

        @pl.when(b != me)
        def _():
            pltpu.make_async_remote_copy(
                src_ref=before_out.at[group(b)],
                dst_ref=before_in.at[group(me)],
                send_sem=back_send.at[b],
                recv_sem=back_recv.at[me],
                device_id={"sp": b},
                device_id_type=MESH,
            ).start()

        @pl.when(b == me)
        def _():
            before_in[group(me)] = before_out[group(me)]

        return tuple(
            states[i] * keep_in[b * own + i][0:1, :] + push_in[b * own + i].astype(f32)
            for i in range(own)
        )

    lax.fori_loop(0, n, scan, tuple(jnp.zeros((size, size), f32) for _ in range(own)))

    def settle(k, carry):
        j = other(k)
        wait_bytes(before_in.at[group(j)], back_recv.at[j])
        return carry

    lax.fori_loop(1, n, settle, 0)

    def close(h, carry):
        cols = columns(h)
        mix = within[:, cols] + lax.dot_general(
            qs[:, cols], before_in[h], (((1,), (1,)), ((), ())), preferred_element_type=f32
        )
        scale = lax.rsqrt(jnp.mean(mix * mix, axis=-1, keepdims=True) + NORM_EPS)
        normed = (mix * scale * gain_ref[...]).astype(bf16).astype(f32)
        gate = og_ref[:, cols].astype(f32)
        out_ref[:, cols] = (normed * (gate / (1.0 + jnp.exp(-gate)))).astype(bf16)
        return carry

    lax.fori_loop(0, heads, close, 0)

    def finish(k, carry):
        j = other(k)
        wait_bytes(push.at[group(j)], push_send.at[k])
        wait_bytes(keep.at[group(j)], keep_send.at[k])
        wait_bytes(before_out.at[group(j)], back_send.at[j])
        return carry

    lax.fori_loop(1, n, finish, 0)


def mixer(q, f, v, og, bound, gain):
    n = lax.axis_size("sp")
    tok, wide = q.shape
    size = gain.shape[1]
    heads = wide // size
    bf16 = jnp.bfloat16
    states = pltpu.VMEM((heads, size, size), bf16)
    keeps = pltpu.VMEM((heads, 8, size), jnp.float32)
    return pl.pallas_call(
        functools.partial(mixer_kernel, n),
        out_shape=jax.ShapeDtypeStruct((tok, wide), bf16),
        in_specs=[VMEM_WHOLE] * 6,
        out_specs=VMEM_WHOLE,
        scratch_shapes=[
            pltpu.VMEM((tok, wide), bf16),
            pltpu.VMEM((tok, wide), bf16),
            pltpu.VMEM((tok, wide), jnp.float32),
            states,
            keeps,
            states,
            keeps,
            states,
            states,
        ]
        + [pltpu.SemaphoreType.DMA((n,))] * 6,
        compiler_params=pltpu.CompilerParams(
            collective_id=3, has_side_effects=True, vmem_limit_bytes=32 * 1024 * 1024
        ),
    )(q, f, v, og, bound, gain)


def project_kernel(
    ndp,
    parts,
    g_ref,
    w_ref,
    res_ref,
    gain_ref,
    hid_ref,
    moe_ref,
    g_in,
    outs,
    proj,
    far_send,
    near_send,
    relay_send,
    g_recv,
    r_send,
    r_recv,
):
    me = lax.axis_index("dp")
    tok, wide = g_ref.shape
    share = w_ref.shape[1]
    ny = ndp // 2
    y, core = lax.div(me, 2), lax.rem(me, 2)
    partner = y * 2 + 1 - core
    piece = wide // parts
    barrier = pltpu.get_barrier_semaphore()
    for k in range(1, ndp):
        pl.semaphore_signal(
            barrier, inc=1, device_id={"dp": lax.rem(me + k, ndp)}, device_id_type=MESH
        )
    pl.semaphore_wait(barrier, ndp - 1)

    def rows(j):
        return pl.ds(pl.multiple_of(j * tok, tok), tok)

    def span(c):
        return pl.ds(c * piece, piece)

    def send(src, owner, c, sem, target):
        pltpu.make_async_remote_copy(
            src_ref=src,
            dst_ref=g_in.at[rows(owner), span(c)],
            send_sem=sem,
            recv_sem=g_recv.at[owner, c],
            device_id={"dp": target},
            device_id_type=MESH,
        ).start()

    for c in range(parts):
        for k in range(1, ny):
            send(g_ref.at[:, span(c)], me, c, far_send.at[k], lax.rem(y + k, ny) * 2 + core)
        send(g_ref.at[:, span(c)], me, c, near_send, partner)

    def arrive(owner, c):
        wait_bytes(g_in.at[rows(owner), span(c)], g_recv.at[owner, c])

    mine = pl.ds(pl.multiple_of(me * share, share), share)

    def multiply(src, owner):
        def tile(i, carry):
            cols = pl.ds(pl.multiple_of(i * 256, 256), 256)
            outs[rows(owner), cols] = jnp.dot(
                src[...], w_ref[:, cols], preferred_element_type=jnp.float32
            ).astype(jnp.bfloat16)
            return carry

        lax.fori_loop(0, share // 256, tile, 0)

    def answer(owner):
        multiply(g_in.at[rows(owner), :], owner)
        pltpu.make_async_remote_copy(
            src_ref=outs.at[rows(owner), :],
            dst_ref=proj.at[:, mine],
            send_sem=r_send.at[owner],
            recv_sem=r_recv.at[me],
            device_id={"dp": owner},
            device_id_type=MESH,
        ).start()

    multiply(g_ref, me)
    proj[:, mine] = outs[rows(me), :]

    for c in range(parts):
        arrive(partner, c)
    answer(partner)

    def source(k):
        return lax.rem(y + ny - k, ny) * 2

    for c in range(parts):
        for k in range(1, ny):
            owner = source(k) + core
            arrive(owner, c)
            send(g_in.at[rows(owner), span(c)], owner, c, relay_send.at[k], partner)
    for k in range(1, ny):
        answer(source(k) + core)
    for k in range(1, ny):
        owner = source(k) + 1 - core
        for c in range(parts):
            arrive(owner, c)
        answer(owner)
    for k in range(1, ndp):
        owner = lax.rem(me + k, ndp)
        cols = pl.ds(pl.multiple_of(owner * share, share), share)
        wait_bytes(proj.at[:, cols], r_recv.at[owner])
    hidden = (res_ref[...].astype(jnp.float32) + proj[...].astype(jnp.float32)).astype(jnp.bfloat16)
    hid_ref[...] = hidden
    hidden_f = hidden.astype(jnp.float32)
    scale = lax.rsqrt(jnp.mean(hidden_f * hidden_f, axis=-1, keepdims=True) + NORM_EPS)
    moe_ref[...] = (hidden_f * scale * gain_ref[...]).astype(jnp.bfloat16)
    for k in range(1, ny):
        wait_bytes(g_ref, far_send.at[k])
        wait_bytes(g_ref, relay_send.at[k])
    wait_bytes(g_ref, near_send)
    for k in range(1, ndp):
        owner = lax.rem(me + k, ndp)
        wait_bytes(outs.at[rows(owner), :], r_send.at[owner])


def project(gated, weight, residual, gain):
    ndp = lax.axis_size("dp")
    tok, wide = gated.shape
    share = weight.shape[1]
    model = residual.shape[1]
    bf16 = jnp.bfloat16
    dma = pltpu.SemaphoreType.DMA
    return pl.pallas_call(
        functools.partial(project_kernel, ndp, GATED_PARTS),
        out_shape=[jax.ShapeDtypeStruct((tok, model), bf16)] * 2,
        in_specs=[VMEM_WHOLE] * 4,
        out_specs=[VMEM_WHOLE] * 2,
        scratch_shapes=[
            pltpu.VMEM((ndp * tok, wide), bf16),
            pltpu.VMEM((ndp * tok, share), bf16),
            pltpu.VMEM((tok, model), bf16),
            dma((ndp,)),
            dma,
            dma((ndp,)),
            dma((ndp, GATED_PARTS)),
            dma((ndp,)),
            dma((ndp,)),
        ],
        compiler_params=pltpu.CompilerParams(
            collective_id=4, has_side_effects=True, vmem_limit_bytes=32 * 1024 * 1024
        ),
    )(gated, weight, residual, gain)


def local(
    queries,
    forget_pre,
    values,
    out_gate,
    lower_bound,
    head_gain,
    residual,
    out_weight,
    ffn_gain,
    routing,
    route_weight,
    expert_gate,
    expert_up,
    expert_down,
):
    _, tok_rows, channels = queries.shape
    model_width = residual.shape[2]
    top_count = routing.shape[2]
    span_sp = lax.axis_size("sp")
    span_dp = lax.axis_size("dp")
    experts = expert_gate.shape[0] * span_sp * span_dp
    cap = max(2, 5 * tok_rows * top_count // (4 * experts))
    nx = span_dp // 2
    nz = span_sp // nx
    per = -(-nz * cap // 16) * 16
    width = min(CHUNK, model_width)
    packed = jnp.concatenate(
        [routing.astype(jnp.float32), route_weight], axis=2
    ).reshape(tok_rows * 2 * top_count)
    shared = lax.all_gather(jnp.concatenate([packed, lower_bound]), "sp", axis=0)
    packed, bound = shared[:, : packed.shape[0]], shared[:, packed.shape[0] :]
    gated = mixer(
        queries[0],
        forget_pre[0],
        values[0],
        out_gate[0],
        bound.reshape(1, channels),
        head_gain[None, :],
    )
    hidden, moe_in = project(gated, out_weight, residual[0], ffn_gain[None, :])
    pick, high, low = routing_tables(
        packed.reshape(span_sp, tok_rows, 2 * top_count),
        nz,
        nx,
        span_dp,
        cap,
        per,
    )
    act = dispatch(moe_in, pick, expert_gate[0], expert_up[0], nz, nx, span_dp, width)
    layer_out = combine(act, expert_down[0], high, low, hidden, nz, nx, span_dp, width)
    return layer_out.reshape(1, tok_rows, model_width)


def solution(mesh):
    in_specs = (
        P("dp", "sp", None),
        P("dp", "sp", None),
        P("dp", "sp", None),
        P("dp", "sp", None),
        P("sp"),
        P(),
        P("dp", "sp", None),
        P(None, "dp"),
        P(),
        P("dp", "sp", None),
        P("dp", "sp", None),
        P(("sp", "dp"), None, None),
        P(("sp", "dp"), None, None),
        P(("sp", "dp"), None, None),
    )
    out_specs = P("dp", "sp", None)
    return jax.shard_map(local, mesh=mesh, in_specs=in_specs, out_specs=out_specs, check_vma=False)
```

profile of v0, /device:TPU:0, one launch (start us, length us, event | category | flops | bytes accessed | tf_op | source)
XLA Modules:
  0.0 292.6 jit_solution(16007083460076467117)
XLA Ops:
  0.0 0.7 convert_element_type.23
  0.7 0.7 pad_maximum_fusion.1
  1.4 0.1 copy.33
  1.6 0.7 pad_maximum_fusion
  2.3 32.5 %all-gather.1 = f32[8,1,1280]{2,1,0:T(1,128)S(1)} all-gather(f32[1,1,1280]{2,1,0:T(1,128)S(1)} %reshape.34), channel_id=2, replica_groups=mesh['sp'=8,'dp'=4] {'sp'}, dimensions={0}, use_global_device_ids=true | all-gather | bytes 46080 | tf_op jit(solution)/shard_map/all_gather | solution.py:837
  34.8 0.3 reshape_reshape.3
  35.1 0.1 copy.34
  35.4 0.2 bitcast_select_fusion.1
  35.6 0.2 eq.64
  35.8 0.1 copy.52
  35.9 0.4 copy.37
  36.4 0.2 broadcast_in_dim.62
  36.6 1.2 copy.51
  37.7 1.7 copy.39
  39.5 1.3 fusion
  40.9 0.2 eq.58
  41.1 1.1 fusion.1.pick_ref
  42.2 27.6 %shard_map.136.g_ref = bf16[128,2048]{1,0:T(8,128)(2,1)S(1)} custom-call(bf16[128,2048]{1,0:T(8,128)(2,1)S(1)} %bitcast.52, bf16[128,2048]{1,0:T(8,128)(2,1)S(1)} %bitcast.53, bf16[128,2048]{1,0:T(8,128)(2,1)S(1)} %bitcast.54, bf16[128,2048]{1,0:T(8,128)(2,1)S(1)} %bitcast.55, f32[1,2048]{1,0:T(1,128)S(1)} %bitcast.56, f32[1,128]{1,0:T(1,128)S(1)} %bitcast.58), custom_call_target="tpu_custom_call" | custom-call | tf_op jit(solution)/shard_map/pallas_call | solution.py:635
  69.8 28.6 %shard_map.137 = (bf16[128,4096]{1,0:T(8,128)(2,1)S(1)}, bf16[128,4096]{1,0:T(8,128)(2,1)S(1)}) custom-call(bf16[128,2048]{1,0:T(8,128)(2,1)S(1)} %shard_map.136.g_ref, bf16[2048,1024]{1,0:T(8,128)(2,1)S(1)} %copy-done, bf16[128,4096]{1,0:T(8,128)(2,1)S(1)} %bitcast.51, f32[1,4096]{1,0:T(1,128)S(1)} %bitcast.57), custom_call_target="tpu_custom_call" | custom-call | tf_op jit(solution)/shard_map/pallas_call | solution.py:785
  98.5 1.0 copy-done.2
  99.4 1.0 copy-done.3
  100.4 95.8 %shard_map.138.act_ref = bf16[640,512]{1,0:T(8,128)(2,1)} custom-call(bf16[128,4096]{1,0:T(8,128)(2,1)} %copy-done.3, bf16[640,512]{1,0:T(8,128)(2,1)} %fusion.1.pick_ref, bf16[4096,512]{1,0:T(8,128)(2,1)} %bitcast.65, bf16[4096,512]{1,0:T(8,128)(2,1)} %bitcast.66), custom_call_target="tpu_custom_call" | custom-call | tf_op jit(solution)/shard_map/pallas_call | solution.py:397
  196.1 94.2 %shard_map.139 = bf16[128,4096]{1,0:T(8,128)(2,1)} custom-call(bf16[640,512]{1,0:T(8,128)(2,1)} %shard_map.138.act_ref, bf16[512,4096]{1,0:T(8,128)(2,1)} %bitcast.64, bf16[512,640]{1,0:T(8,128)(2,1)} %get-tuple-element.10.high_ref, bf16[512,640]{1,0:T(8,128)(2,1)} %get-tuple-element.9.low_ref, bf16[128,4096]{1,0:T(8,128)(2,1)} %copy-done.2), custom_call_target="tpu_custom_call" | custom-call | tf_op jit(solution)/shard_map/pallas_call | solution.py:426
  290.3 2.3 copy.55
  (37 shorter events, 0.5 us)
Async XLA Ops:
  39.5 2.6 copy-start.5
  39.5 2.6 copy-start.6
  39.5 2.6 copy-start.7
  40.9 1.3 copy-start.4
  40.9 29.0 %copy-start.1 = (bf16[1,128,4096]{2,1,0:T(8,128)(2,1)S(1)}, bf16[1,128,4096]{2,1,0:T(8,128)(2,1)}, u32[]{:S(2)}) copy-start(bf16[1,128,4096]{2,1,0:T(8,128)(2,1)} %param.20) | copy-start | bytes 3145732
  41.1 1.1 copy-start.9
  41.1 28.8 %copy-start = (bf16[2048,1024]{1,0:T(8,128)(2,1)S(1)}, bf16[2048,1024]{1,0:T(8,128)(2,1)}, u32[]{:S(2)}) copy-start(bf16[2048,1024]{1,0:T(8,128)(2,1)} %w_ref.1) | copy-start | bytes 12582916
  42.2 27.6 %copy-start.8 = (f32[4096]{0:T(1024)S(1)}, f32[4096]{0:T(1024)}, u32[]{:S(2)}) copy-start(f32[4096]{0:T(1024)} %param.22) | copy-start | bytes 49156
  98.4 1.0 copy-start.2
  99.4 1.0 copy-start.3
where the time goes:
time: 294 us; the launch traced here: 293 us
  Pallas kernels  246 us (84%)
  blocking collectives  32.5 us (11%)
  local copies, waits for them, and re-layouts  8.89 us (3%)
  other arithmetic  4.62 us (2%)
    pallas_call x1, Pallas kernels, dispatch(): pl.pallas_call(functools.partial(dispatch_kernel, nz, nx, ndp, width), ou...  95.8 us
    pallas_call x1, Pallas kernels, combine(): pl.pallas_call(functools.partial(return_kernel, nz, nx, ndp, width), out_...  94.2 us
    all_gather x1, blocking collectives, local(): lax.all_gather(jnp.concatenate([packed, lower_bound]), 'sp', axis=0)  32.5 us
    pallas_call x1, Pallas kernels, project(): pl.pallas_call(functools.partial(project_kernel, ndp, GATED_PARTS), out_s...  28.6 us
    pallas_call x1, Pallas kernels, mixer(): pl.pallas_call(functools.partial(mixer_kernel, n), out_shape=jax.ShapeDty...  27.6 us

commit v1 on v0

--- a/solution.py
+++ b/solution.py
@@ -10,7 +10,7 @@
 MESH = pl.DeviceIdType.MESH
 VMEM_WHOLE = pl.BlockSpec(memory_space=pltpu.VMEM)
 
-CHUNK = 512
+CHUNK = 256
 GATED_PARTS = 4
 
 
@@ -55,16 +55,44 @@
     pl.semaphore_wait(barrier, count)
 
 
+def routing_tables(packed_ref, nz, nx, ndp, cap):
+    peers = nx * ndp
+    _, double, tok = packed_ref.shape
+    top = double // 2
+    sp = lax.axis_index("sp")
+    z, x = lax.div(sp, nx), lax.rem(sp, nx)
+    ids = lax.broadcasted_iota(jnp.int32, (peers, tok), 0) + z * peers
+    row = lax.broadcasted_iota(jnp.int32, (tok, tok), 0)
+    col = lax.broadcasted_iota(jnp.int32, (tok, tok), 1)
+    earlier = jnp.where(row < col, 1.0, 0.0).astype(jnp.bfloat16)
+    found = []
+    for b in range(nz):
+        item = packed_ref[b * nx + x]
+        chosen = item[:top].astype(jnp.int32)
+        named = jnp.zeros((peers, tok), jnp.float32)
+        weight = jnp.zeros((peers, tok), jnp.float32)
+        for j in range(top):
+            same = chosen[j : j + 1] == ids
+            named = jnp.where(same, 1.0, named)
+            weight = jnp.where(same, item[top + j : top + j + 1], weight)
+        rank = jnp.dot(named.astype(jnp.bfloat16), earlier, preferred_element_type=jnp.float32)
+        slot = jnp.where(named > 0, b * cap + rank.astype(jnp.int32), -1)
+        found.append((slot, weight))
+    return found
+
+
 def dispatch_kernel(
     nz,
     nx,
     ndp,
     width,
+    cap,
     x_ref,
-    pick_ref,
+    packed_ref,
     gate_ref,
     lift_ref,
     act_ref,
+    pick_ref,
     gath,
     slots,
     got,
@@ -100,6 +128,12 @@
         ).start()
 
     gath[block(z), :] = x_ref[...]
+    slot_ids = lax.broadcasted_iota(jnp.int32, (per, tok), 0)
+    for b, (slot, _) in enumerate(routing_tables(packed_ref, nz, nx, ndp, cap)):
+        for p in range(peers):
+            pick_ref[p * per : (p + 1) * per, b * tok : (b + 1) * tok] = jnp.where(
+                slot_ids == slot[p : p + 1], 1.0, 0.0
+            ).astype(jnp.bfloat16)
     gate_sum[...] = jnp.zeros_like(gate_sum)
     lift_sum[...] = jnp.zeros_like(lift_sum)
 
@@ -208,12 +242,15 @@
     nx,
     ndp,
     width,
+    cap,
     act_ref,
     down_ref,
+    packed_ref,
+    h_ref,
+    out_ref,
+    mixed,
     high_ref,
     low_ref,
-    h_ref,
-    out_ref,
     r_ref,
     ret,
     part,
@@ -265,10 +302,20 @@
 
     lax.fori_loop(0, chunks, send_chunk, 0)
     ret[share(me), :] = r_ref[share(me), :]
-
-    def line(c, first, sends, takes, inbox, outbox, send_sem, recv_sem, device):
+    slot_ids = lax.broadcasted_iota(jnp.int32, (per, tok), 0)
+    for b, (slot, weight) in enumerate(routing_tables(packed_ref, nz, nx, ndp, cap)):
+        for p in range(peers):
+            mixed[p * per : (p + 1) * per, b * tok : (b + 1) * tok] = jnp.where(
+                slot_ids == slot[p : p + 1], weight[p : p + 1], 0.0
+            )
+    turned = mixed[...].T
+    high = turned.astype(jnp.bfloat16)
+    high_ref[...] = high
+    low_ref[...] = (turned - high.astype(jnp.float32)).astype(jnp.bfloat16)
+
+    def line(order, c, first, sends, takes, inbox, outbox, send_sem, recv_sem, device):
         cols = columns(c)
-        for d in range(nz):
+        for d in order:
             rows = pl.ds(d * tok, tok)
 
             @pl.when(jnp.logical_not(first) & takes(d))
@@ -317,7 +364,16 @@
         @pl.when((cu >= 0) & (cu < chunks))
         def _():
             line(
-                cu, z == 0, lambda d: d > z, lambda d: d >= z, up_in, up_out, up_send, up_recv, above
+                range(nz - 1, -1, -1),
+                cu,
+                z == 0,
+                lambda d: d > z,
+                lambda d: d >= z,
+                up_in,
+                up_out,
+                up_send,
+                up_recv,
+                above,
             )
 
         cd = t - (nz - 1 - z)
@@ -325,7 +381,16 @@
         @pl.when((cd >= 0) & (cd < chunks))
         def _():
             line(
-                cd, z == nz - 1, lambda d: d < z, lambda d: d <= z, dn_in, dn_out, dn_send, dn_recv, below
+                range(nz),
+                cd,
+                z == nz - 1,
+                lambda d: d < z,
+                lambda d: d <= z,
+                dn_in,
+                dn_out,
+                dn_send,
+                dn_recv,
+                below,
             )
 
         return carry
@@ -361,45 +426,20 @@
     lax.fori_loop(1, peers, finish, 0)
 
 
-def routing_tables(packed, nz, nx, ndp, cap, per):
-    tok, top = packed.shape[1], packed.shape[2] // 2
-    peers = nx * ndp
-    sp = lax.axis_index("sp")
-    z, x = sp // nx, sp % nx
-    packed = lax.dynamic_index_in_dim(packed.reshape(nz, nx, tok, 2 * top), x, 1, keepdims=False)
-    chosen = packed[..., :top].astype(jnp.int32)
-    experts = z * peers + jnp.arange(peers, dtype=jnp.int32)
-    same = chosen[:, :, :, None] == experts
-    named = jnp.any(same, axis=2)
-    weight = jnp.sum(jnp.where(same, packed[..., top:, None], 0.0), axis=2)
-    earlier = jnp.tril(jnp.ones((tok, tok), jnp.bfloat16), -1)
-    rank = jnp.einsum(
-        "ts,bsp->btp", earlier, named.astype(jnp.bfloat16), preferred_element_type=jnp.float32
-    ).astype(jnp.int32)
-    slot = jnp.arange(nz, dtype=jnp.int32)[:, None, None] * cap + rank
-    slot = jnp.where(named, slot, per)
-    slot_ids = jnp.arange(per, dtype=jnp.int32)
-    pick = slot.transpose(2, 0, 1)[:, None, :, :] == slot_ids[None, :, None, None]
-    pick = pick.astype(jnp.bfloat16).reshape(peers * per, nz * tok)
-    mixed = jnp.where(slot[..., None] == slot_ids, weight[..., None], 0.0)
-    mixed = mixed.reshape(nz * tok, peers * per)
-    high = lax.reduce_precision(mixed, 8, 7)
-    return pick, high.astype(jnp.bfloat16), (mixed - high).astype(jnp.bfloat16)
-
-
-def dispatch(moe_in, pick, w_gate, w_up, nz, nx, ndp, width):
+def dispatch(moe_in, packed, w_gate, w_up, nz, nx, ndp, width, cap, per):
     tok, model = moe_in.shape
     inner = w_gate.shape[1]
     peers = nx * ndp
-    total = pick.shape[0]
+    total = peers * per
     chunks = model // width
     bf16 = jnp.bfloat16
     return pl.pallas_call(
-        functools.partial(dispatch_kernel, nz, nx, ndp, width),
+        functools.partial(dispatch_kernel, nz, nx, ndp, width, cap),
         out_shape=jax.ShapeDtypeStruct((total, inner), bf16),
         in_specs=[VMEM_WHOLE] * 4,
         out_specs=VMEM_WHOLE,
         scratch_shapes=[
+            pltpu.VMEM((total, nz * tok), bf16),
             pltpu.VMEM((nz * tok, model), bf16),
             pltpu.VMEM((total, model), bf16),
             pltpu.VMEM((total, model), bf16),
@@ -414,21 +454,24 @@
         compiler_params=pltpu.CompilerParams(
             collective_id=1, has_side_effects=True, vmem_limit_bytes=60 * 1024 * 1024
         ),
-    )(moe_in, pick, w_gate, w_up)
-
-
-def combine(act, w_down, high, low, hidden, nz, nx, ndp, width):
+    )(moe_in, packed, w_gate, w_up)
+
+
+def combine(act, w_down, packed, hidden, nz, nx, ndp, width, cap):
     tok, model = hidden.shape
     peers = nx * ndp
     total = act.shape[0]
     chunks = model // width
     bf16 = jnp.bfloat16
     return pl.pallas_call(
-        functools.partial(return_kernel, nz, nx, ndp, width),
+        functools.partial(return_kernel, nz, nx, ndp, width, cap),
         out_shape=jax.ShapeDtypeStruct((tok, model), bf16),
-        in_specs=[VMEM_WHOLE] * 5,
+        in_specs=[VMEM_WHOLE] * 4,
         out_specs=VMEM_WHOLE,
         scratch_shapes=[
+            pltpu.VMEM((total, nz * tok), jnp.float32),
+            pltpu.VMEM((nz * tok, total), bf16),
+            pltpu.VMEM((nz * tok, total), bf16),
             pltpu.VMEM((total, model), bf16),
             pltpu.VMEM((total, model), bf16),
             pltpu.VMEM((nz * tok, model), jnp.float32),
@@ -446,7 +489,7 @@
         compiler_params=pltpu.CompilerParams(
             collective_id=2, has_side_effects=True, vmem_limit_bytes=60 * 1024 * 1024
         ),
-    )(act, w_down, high, low, hidden)
+    )(act, w_down, packed, hidden)
 
 
 def mixer_kernel(
@@ -455,11 +498,16 @@
     f_ref,
     v_ref,
     og_ref,
-    bound_ref,
+    own_bound_ref,
+    own_pack_ref,
     gain_ref,
     out_ref,
+    pack_ref,
+    bound_in,
     qs,
+    qr,
     ks,
+    kr,
     within,
     push,
     keep,
@@ -467,6 +515,10 @@
     keep_in,
     before_out,
     before_in,
+    bound_send,
+    pack_send,
+    bound_recv,
+    pack_recv,
     push_send,
     keep_send,
     push_recv,
@@ -490,6 +542,27 @@
 
     lax.fori_loop(1, n, greet_one, 0)
 
+    bound_in[me] = own_bound_ref[...]
+    pack_ref[me] = own_pack_ref[...]
+    pl.semaphore_wait(barrier, n - 1)
+
+    def spread(k, carry):
+        for src, dst, send_sem, recv_sem in (
+            (own_bound_ref, bound_in, bound_send, bound_recv),
+            (own_pack_ref, pack_ref, pack_send, pack_recv),
+        ):
+            pltpu.make_async_remote_copy(
+                src_ref=src,
+                dst_ref=dst.at[me],
+                send_sem=send_sem.at[k],
+                recv_sem=recv_sem.at[me],
+                device_id={"sp": other(k)},
+                device_id_type=MESH,
+            ).start()
+        return carry
+
+    lax.fori_loop(1, n, spread, 0)
+
     row = lax.broadcasted_iota(jnp.int32, (tok, tok), 0)
     col = lax.broadcasted_iota(jnp.int32, (tok, tok), 1)
     causal = row >= col
@@ -501,32 +574,42 @@
     def group(j):
         return pl.ds(j * own, own)
 
-    def prepare(h, carry):
-        cols = columns(h)
-        forget = f_ref[:, cols].astype(f32)
-        leak = (1.0 - bound_ref[:, cols]) / (1.0 + jnp.exp(forget))
-        log_keep = jnp.log1p(-leak)
-        first = log_keep.astype(bf16)
-        rest = log_keep - first.astype(f32)
-        second = rest.astype(bf16)
-        third = (rest - second.astype(f32)).astype(bf16)
-        log_run = (
-            jnp.dot(lower, first, preferred_element_type=f32)
-            + jnp.dot(lower, second, preferred_element_type=f32)
-            + jnp.dot(lower, third, preferred_element_type=f32)
-        )
-        last = log_run[tok - 1 : tok, :]
-        ks[:, cols] = (leak * jnp.exp(-log_run)).astype(bf16)
-        qs[:, cols] = (q_ref[:, cols].astype(f32) * jnp.exp(log_run)).astype(bf16)
-        carry_key = (leak * jnp.exp(last - log_run)).astype(bf16)
-        push[h] = lax.dot_general(
-            v_ref[:, cols], carry_key, (((0,), (0,)), ((), ())), preferred_element_type=f32
-        ).astype(bf16)
-        keep[h] = jnp.broadcast_to(jnp.exp(last), (8, size))
-        return carry
-
-    lax.fori_loop(0, heads, prepare, 0)
-    pl.semaphore_wait(barrier, n - 1)
+    def halves(value):
+        first = value.astype(bf16)
+        return first, (value - first.astype(f32)).astype(bf16)
+
+    def prepare(j, carry):
+        @pl.when(j != me)
+        def _():
+            wait_bytes(bound_in.at[j], bound_recv.at[j])
+
+        for i in range(own):
+            h = j * own + i
+            cols = columns(h)
+            bound = bound_in[j][:, i * size : (i + 1) * size]
+            forget = f_ref[:, cols].astype(f32)
+            leak = (1.0 - bound) / (1.0 + jnp.exp(forget))
+            log_keep = jnp.log1p(-leak)
+            first = log_keep.astype(bf16)
+            second, third = halves(log_keep - first.astype(f32))
+            log_run = (
+                jnp.dot(lower, first, preferred_element_type=f32)
+                + jnp.dot(lower, second, preferred_element_type=f32)
+                + jnp.dot(lower, third, preferred_element_type=f32)
+            )
+            last = log_run[tok - 1 : tok, :]
+            ks[:, cols], kr[:, cols] = halves(leak * jnp.exp(-log_run))
+            qs[:, cols], qr[:, cols] = halves(q_ref[:, cols].astype(f32) * jnp.exp(log_run))
+            total = jnp.zeros((size, size), f32)
+            for term in halves(leak * jnp.exp(last - log_run)):
+                total = total + lax.dot_general(
+                    v_ref[:, cols], term, (((0,), (0,)), ((), ())), preferred_element_type=f32
+                )
+            push[h] = total.astype(bf16)
+            keep[h] = jnp.broadcast_to(jnp.exp(last), (8, size))
+        return carry
+
+    lax.fori_loop(0, n, prepare, 0)
 
     def send_push(k, carry):
         j = other(k)
@@ -552,16 +635,24 @@
     push_in[group(me)] = push[group(me)]
     keep_in[group(me)] = keep[group(me)]
 
-    def inside(h, carry):
-        cols = columns(h)
-        scores = lax.dot_general(
-            qs[:, cols], ks[:, cols], (((1,), (1,)), ((), ())), preferred_element_type=f32
-        )
-        scores = jnp.where(causal, scores, 0.0).astype(bf16)
-        within[:, cols] = jnp.dot(scores, v_ref[:, cols], preferred_element_type=f32)
-        return carry
-
-    lax.fori_loop(0, heads, inside, 0)
+    def across(a, b):
+        return lax.dot_general(a, b, (((1,), (1,)), ((), ())), preferred_element_type=f32)
+
+    def inside(j, carry):
+        for i in range(own):
+            cols = columns(j * own + i)
+            scores = (
+                across(qs[:, cols], ks[:, cols])
+                + across(qs[:, cols], kr[:, cols])
+                + across(qr[:, cols], ks[:, cols])
+            )
+            first, second = halves(jnp.where(causal, scores, 0.0))
+            within[:, cols] = jnp.dot(
+                first, v_ref[:, cols], preferred_element_type=f32
+            ) + jnp.dot(second, v_ref[:, cols], preferred_element_type=f32)
+        return carry
+
+    lax.fori_loop(0, n, inside, 0)
 
     def scan(b, states):
         @pl.when(b != me)
@@ -601,21 +692,28 @@
 
     lax.fori_loop(1, n, settle, 0)
 
-    def close(h, carry):
-        cols = columns(h)
-        mix = within[:, cols] + lax.dot_general(
-            qs[:, cols], before_in[h], (((1,), (1,)), ((), ())), preferred_element_type=f32
-        )
-        scale = lax.rsqrt(jnp.mean(mix * mix, axis=-1, keepdims=True) + NORM_EPS)
-        normed = (mix * scale * gain_ref[...]).astype(bf16).astype(f32)
-        gate = og_ref[:, cols].astype(f32)
-        out_ref[:, cols] = (normed * (gate / (1.0 + jnp.exp(-gate)))).astype(bf16)
-        return carry
-
-    lax.fori_loop(0, heads, close, 0)
+    def close(j, carry):
+        for i in range(own):
+            h = j * own + i
+            cols = columns(h)
+            mix = (
+                within[:, cols]
+                + across(qs[:, cols], before_in[h])
+                + across(qr[:, cols], before_in[h])
+            )
+            scale = lax.rsqrt(jnp.mean(mix * mix, axis=-1, keepdims=True) + NORM_EPS)
+            normed = (mix * scale * gain_ref[...]).astype(bf16).astype(f32)
+            gate = og_ref[:, cols].astype(f32)
+            out_ref[:, cols] = (normed * (gate / (1.0 + jnp.exp(-gate)))).astype(bf16)
+        return carry
+
+    lax.fori_loop(0, n, close, 0)
 
     def finish(k, carry):
         j = other(k)
+        wait_bytes(pack_ref.at[j], pack_recv.at[j])
+        wait_bytes(own_pack_ref, pack_send.at[k])
+        wait_bytes(own_bound_ref, bound_send.at[k])
         wait_bytes(push.at[group(j)], push_send.at[k])
         wait_bytes(keep.at[group(j)], keep_send.at[k])
         wait_bytes(before_out.at[group(j)], back_send.at[j])
@@ -624,7 +722,7 @@
     lax.fori_loop(1, n, finish, 0)
 
 
-def mixer(q, f, v, og, bound, gain):
+def mixer(q, f, v, og, bound, pack, gain):
     n = lax.axis_size("sp")
     tok, wide = q.shape
     size = gain.shape[1]
@@ -634,10 +732,16 @@
     keeps = pltpu.VMEM((heads, 8, size), jnp.float32)
     return pl.pallas_call(
         functools.partial(mixer_kernel, n),
-        out_shape=jax.ShapeDtypeStruct((tok, wide), bf16),
-        in_specs=[VMEM_WHOLE] * 6,
-        out_specs=VMEM_WHOLE,
+        out_shape=[
+            jax.ShapeDtypeStruct((tok, wide), bf16),
+            jax.ShapeDtypeStruct((n,) + pack.shape, jnp.float32),
+        ],
+        in_specs=[VMEM_WHOLE] * 7,
+        out_specs=[VMEM_WHOLE] * 2,
         scratch_shapes=[
+            pltpu.VMEM((n,) + bound.shape, jnp.float32),
+            pltpu.VMEM((tok, wide), bf16),
+            pltpu.VMEM((tok, wide), bf16),
             pltpu.VMEM((tok, wide), bf16),
             pltpu.VMEM((tok, wide), bf16),
             pltpu.VMEM((tok, wide), jnp.float32),
@@ -648,11 +752,11 @@
             states,
             states,
         ]
-        + [pltpu.SemaphoreType.DMA((n,))] * 6,
+        + [pltpu.SemaphoreType.DMA((n,))] * 10,
         compiler_params=pltpu.CompilerParams(
             collective_id=3, has_side_effects=True, vmem_limit_bytes=32 * 1024 * 1024
         ),
-    )(q, f, v, og, bound, gain)
+    )(q, f, v, og, bound, pack, gain)
 
 
 def project_kernel(
@@ -820,7 +924,7 @@
     expert_up,
     expert_down,
 ):
-    _, tok_rows, channels = queries.shape
+    tok_rows = queries.shape[1]
     model_width = residual.shape[2]
     top_count = routing.shape[2]
     span_sp = lax.axis_size("sp")
@@ -831,30 +935,21 @@
     nz = span_sp // nx
     per = -(-nz * cap // 16) * 16
     width = min(CHUNK, model_width)
-    packed = jnp.concatenate(
-        [routing.astype(jnp.float32), route_weight], axis=2
-    ).reshape(tok_rows * 2 * top_count)
-    shared = lax.all_gather(jnp.concatenate([packed, lower_bound]), "sp", axis=0)
-    packed, bound = shared[:, : packed.shape[0]], shared[:, packed.shape[0] :]
-    gated = mixer(
+    pack = jnp.concatenate([routing[0].astype(jnp.float32), route_weight[0]], axis=1).T
+    gated, packed = mixer(
         queries[0],
         forget_pre[0],
         values[0],
         out_gate[0],
-        bound.reshape(1, channels),
+        lower_bound[None, :],
+        pack,
         head_gain[None, :],
     )
     hidden, moe_in = project(gated, out_weight, residual[0], ffn_gain[None, :])
-    pick, high, low = routing_tables(
-        packed.reshape(span_sp, tok_rows, 2 * top_count),
-        nz,
-        nx,
-        span_dp,
-        cap,
-        per,
+    act = dispatch(
+        moe_in, packed, expert_gate[0], expert_up[0], nz, nx, span_dp, width, cap, per
     )
-    act = dispatch(moe_in, pick, expert_gate[0], expert_up[0], nz, nx, span_dp, width)
-    layer_out = combine(act, expert_down[0], high, low, hidden, nz, nx, span_dp, width)
+    layer_out = combine(act, expert_down[0], packed, hidden, nz, nx, span_dp, width, cap)
     return layer_out.reshape(1, tok_rows, model_width)
 
 

time: 294 us -> 270 us (0.918)
  blocking collectives: 32.5 us -> 0 us
  Pallas kernels: 246 us -> 253 us
  local copies, waits for them, and re-layouts: 8.89 us -> 14.4 us
  other arithmetic: 4.62 us -> 1.37 us
    all_gather x1 -> x0, blocking collectives: 32.5 us -> none  [local(): lax.all_gather(jnp.concatenate([packed, lower_bound]), 'sp', axis=0)]
    unnamed x27 -> x25, local copies, waits for them, and re-layouts: 5.54 us -> 14.4 us
    pallas_call x3, Pallas kernels: 218 us -> 225 us  [the longest x1 93.2 us: dispatch(): pl.pallas_call(functools.partial(dispatch_kernel, nz, nx, ndp, width, cap...]
where the time goes in v1:
time: 270 us; the launch traced here: 269 us
  Pallas kernels  253 us (94%)
  local copies, waits for them, and re-layouts  14.4 us (5%)
    pallas_call x1, Pallas kernels, dispatch(): pl.pallas_call(functools.partial(dispatch_kernel, nz, nx, ndp, width, cap...  93.2 us
    pallas_call x1, Pallas kernels, combine(): pl.pallas_call(functools.partial(return_kernel, nz, nx, ndp, width, cap),...  92 us
    pallas_call x1, Pallas kernels, mixer(): pl.pallas_call(functools.partial(mixer_kernel, n), out_shape=[jax.ShapeDt...  39.6 us
    pallas_call x1, Pallas kernels, project(): pl.pallas_call(functools.partial(project_kernel, ndp, GATED_PARTS), out_s...  28.5 us
    unnamed x25, local copies, waits for them, and re-layouts  14.4 us

profile of v1, /device:TPU:0, one launch (start us, length us, event | category | flops | bytes accessed | tf_op | source)
XLA Modules:
  0.0 269.2 jit_solution(12606612834042515612)
XLA Ops:
  0.0 0.7 convert_bitcast_fusion
  0.7 0.7 maximum_bitcast_fusion.own_pack_ref
  1.4 0.0 copy-start.4
  1.4 1.0 copy-done.4
  2.4 0.0 copy-start.5
  2.4 1.0 copy-done.5
  3.5 0.0 copy-start.6
  3.5 1.0 copy-done.6
  4.5 1.0 copy-done.7
  5.5 0.7 copy-done.10
  6.2 0.7 copy-done.11
  6.9 39.6 %shard_map.136 = (bf16[128,2048]{1,0:T(8,128)(2,1)S(1)}, f32[8,8,128]{2,1,0:T(8,128)S(1)}) custom-call(bf16[128,2048]{1,0:T(8,128)(2,1)S(1)} %bitcast.18, bf16[128,2048]{1,0:T(8,128)(2,1)S(1)} %bitcast.19, bf16[128,2048]{1,0:T(8,128)(2,1)S(1)} %bitcast.20, bf16[128,2048]{1,0:T(8,128)(2,1)S(1)} %bitcast.21, f32[1,256]{1,0:T(1,128)S(1)} %bitcast.23, ...), custom_call_target="tpu_custom_call" | custom-call | tf_op jit(solution)/shard_map/pallas_call | solution.py:733
  46.5 0.0 copy-start.8
  46.5 0.6 copy-done.8
  47.1 2.2 copy-done
  49.2 1.2 copy-done.2
  50.5 0.7 copy-done.9
  51.2 28.5 %shard_map.137 = (bf16[128,4096]{1,0:T(8,128)(2,1)S(1)}, bf16[128,4096]{1,0:T(8,128)(2,1)S(1)}) custom-call(bf16[128,2048]{1,0:T(8,128)(2,1)S(1)} %get-tuple-element.9.g_ref, bf16[2048,1024]{1,0:T(8,128)(2,1)S(1)} %copy-done, bf16[128,4096]{1,0:T(8,128)(2,1)S(1)} %bitcast.17, f32[1,4096]{1,0:T(1,128)S(1)} %bitcast.22), custom_call_target="tpu_custom_call" | custom-call | tf_op jit(solution)/shard_map/pallas_call | solution.py:889
  79.7 0.0 copy-start.1
  79.7 1.0 copy-done.1
  80.7 1.0 copy-done.3
  81.6 93.2 %shard_map.138.act_ref = bf16[640,512]{1,0:T(8,128)(2,1)} custom-call(bf16[128,4096]{1,0:T(8,128)(2,1)} %copy-done.1, f32[8,8,128]{2,1,0:T(8,128)} %copy-done.8, bf16[4096,512]{1,0:T(8,128)(2,1)} %bitcast.25, bf16[4096,512]{1,0:T(8,128)(2,1)} %bitcast.26), custom_call_target="tpu_custom_call" | custom-call | tf_op jit(solution)/shard_map/pallas_call | solution.py:436
  174.9 92.0 %shard_map.139 = bf16[128,4096]{1,0:T(8,128)(2,1)} custom-call(bf16[640,512]{1,0:T(8,128)(2,1)} %shard_map.138.act_ref, bf16[512,4096]{1,0:T(8,128)(2,1)} %bitcast.27, f32[8,8,128]{2,1,0:T(8,128)} %copy-done.8, bf16[128,4096]{1,0:T(8,128)(2,1)} %copy-done.3), custom_call_target="tpu_custom_call" | custom-call | tf_op jit(solution)/shard_map/pallas_call | solution.py:466
  266.9 2.3 copy.16
  (7 shorter events, 0.0 us)
Async XLA Ops:
  1.4 1.0 copy-start.4
  2.4 1.0 copy-start.5
  3.5 1.0 copy-start.6
  4.5 1.0 copy-start.7
  5.5 0.7 copy-start.10
  6.2 0.7 copy-start.11
  46.5 0.6 copy-start.8
  47.1 2.2 copy-start
  49.2 1.2 copy-start.2
  50.5 0.7 copy-start.9
  79.7 1.0 copy-start.1
  80.7 1.0 copy-start.3

commit v2 on v1

--- a/solution.py
+++ b/solution.py
@@ -454,6 +454,7 @@
         compiler_params=pltpu.CompilerParams(
             collective_id=1, has_side_effects=True, vmem_limit_bytes=60 * 1024 * 1024
         ),
+        cost_estimate=spent(6 * total * model * inner, total * model * nz),
     )(moe_in, packed, w_gate, w_up)
 
 
@@ -489,7 +490,12 @@
         compiler_params=pltpu.CompilerParams(
             collective_id=2, has_side_effects=True, vmem_limit_bytes=60 * 1024 * 1024
         ),
+        cost_estimate=spent(6 * nz * tok * total * model, total * model * nz),
     )(act, w_down, packed, hidden)
+
+
+def spent(flops, moved):
+    return pl.CostEstimate(flops=4 * flops, bytes_accessed=16 * moved, transcendentals=0)
 
 
 def mixer_kernel(
@@ -756,6 +762,7 @@
         compiler_params=pltpu.CompilerParams(
             collective_id=3, has_side_effects=True, vmem_limit_bytes=32 * 1024 * 1024
         ),
+        cost_estimate=spent(24 * tok * wide * size, 8 * tok * wide),
     )(q, f, v, og, bound, pack, gain)
 
 
@@ -905,6 +912,7 @@
         compiler_params=pltpu.CompilerParams(
             collective_id=4, has_side_effects=True, vmem_limit_bytes=32 * 1024 * 1024
         ),
+        cost_estimate=spent(2 * ndp * tok * wide * share, 2 * wide * share),
     )(gated, weight, residual, gain)
 
 

time: 270 us -> 265 us (0.981)
  local copies, waits for them, and re-layouts: 14.4 us -> 9.73 us
    unnamed x25, local copies, waits for them, and re-layouts: 14.4 us -> 9.73 us
where the time goes in v2:
time: 265 us
  Pallas kernels  253 us (95%)
  local copies, waits for them, and re-layouts  9.73 us (4%)
    pallas_call x1, Pallas kernels, dispatch(): pl.pallas_call(functools.partial(dispatch_kernel, nz, nx, ndp, width, cap...  93.2 us
    pallas_call x1, Pallas kernels, combine(): pl.pallas_call(functools.partial(return_kernel, nz, nx, ndp, width, cap),...  92 us
    pallas_call x1, Pallas kernels, mixer(): pl.pallas_call(functools.partial(mixer_kernel, n), out_shape=[jax.ShapeDt...  39.6 us
    pallas_call x1, Pallas kernels, project(): pl.pallas_call(functools.partial(project_kernel, ndp, GATED_PARTS), out_s...  28.6 us
    unnamed x25, local copies, waits for them, and re-layouts  9.73 us

profile of v2, /device:TPU:0, one launch (start us, length us, event | category | flops | bytes accessed | tf_op | source)
XLA Modules:
  0.0 264.6 jit_solution(17423225898312735553)
XLA Ops:
  0.0 0.7 convert_bitcast_fusion
  0.7 0.7 maximum_bitcast_fusion.own_pack_ref
  1.4 0.0 copy-start.2
  1.4 1.0 copy-done.2
  2.4 0.0 copy-start.3
  2.4 1.0 copy-done.3
  3.5 0.0 copy-start.4
  3.5 1.0 copy-done.4
  4.5 1.0 copy-done.5
  5.5 0.7 copy-done.7
  6.2 0.7 copy-done.8
  6.9 39.6 %shard_map.136 = (bf16[128,2048]{1,0:T(8,128)(2,1)S(1)}, f32[8,8,128]{2,1,0:T(8,128)S(1)}) custom-call(bf16[128,2048]{1,0:T(8,128)(2,1)S(1)} %bitcast.18, bf16[128,2048]{1,0:T(8,128)(2,1)S(1)} %bitcast.19, bf16[128,2048]{1,0:T(8,128)(2,1)S(1)} %bitcast.20, bf16[128,2048]{1,0:T(8,128)(2,1)S(1)} %bitcast.21, f32[1,256]{1,0:T(1,128)S(1)} %bitcast.23, ...), custom_call_target="tpu_custom_call" | custom-call | flops 3221225472 | bytes 33554432 | tf_op jit(solution)/shard_map/pallas_call | solution.py:739
  46.5 0.0 copy-start.11
  46.5 0.0 copy-done
  46.5 0.0 copy-done.1
  46.5 0.0 copy-done.6
  46.5 28.6 %shard_map.137 = (bf16[128,4096]{1,0:T(8,128)(2,1)S(1)}, bf16[128,4096]{1,0:T(8,128)(2,1)S(1)}) custom-call(bf16[128,2048]{1,0:T(8,128)(2,1)S(1)} %get-tuple-element.9.g_ref, bf16[2048,1024]{1,0:T(8,128)(2,1)S(1)} %copy-done, bf16[128,4096]{1,0:T(8,128)(2,1)S(1)} %bitcast.17, f32[1,4096]{1,0:T(1,128)S(1)} %bitcast.22), custom_call_target="tpu_custom_call" | custom-call | flops 8589934592 | bytes 67108864 | tf_op jit(solution)/shard_map/pallas_call | solution.py:896
  75.1 0.0 copy-done.11
  75.1 0.0 copy-start.9
  75.1 1.0 copy-done.9
  76.1 1.0 copy-done.10
  77.0 93.2 %shard_map.138.act_ref = bf16[640,512]{1,0:T(8,128)(2,1)} custom-call(bf16[128,4096]{1,0:T(8,128)(2,1)} %copy-done.10, f32[8,8,128]{2,1,0:T(8,128)} %copy-done.11, bf16[4096,512]{1,0:T(8,128)(2,1)} %bitcast.27, bf16[4096,512]{1,0:T(8,128)(2,1)} %bitcast.28), custom_call_target="tpu_custom_call" | custom-call | flops 32212254720 | bytes 167772160 | tf_op jit(solution)/shard_map/pallas_call | solution.py:436
  170.2 92.0 %shard_map.139 = bf16[128,4096]{1,0:T(8,128)(2,1)} custom-call(bf16[640,512]{1,0:T(8,128)(2,1)} %shard_map.138.act_ref, bf16[512,4096]{1,0:T(8,128)(2,1)} %bitcast.29, f32[8,8,128]{2,1,0:T(8,128)} %copy-done.11, bf16[128,4096]{1,0:T(8,128)(2,1)} %copy-done.9), custom_call_target="tpu_custom_call" | custom-call | flops 32212254720 | bytes 167772160 | tf_op jit(solution)/shard_map/pallas_call | solution.py:467
  262.3 2.3 copy.16
  (7 shorter events, 0.0 us)
Async XLA Ops:
  1.4 1.0 copy-start.2
  2.4 1.0 copy-start.3
  3.5 1.0 copy-start.4
  4.5 1.0 copy-start.5
  5.5 0.7 copy-start.7
  6.2 0.7 copy-start.8
  6.9 39.6 %copy-start = (bf16[2048,1024]{1,0:T(8,128)(2,1)S(1)}, bf16[2048,1024]{1,0:T(8,128)(2,1)}, u32[]{:S(2)}) copy-start(bf16[2048,1024]{1,0:T(8,128)(2,1)} %w_ref.1) | copy-start | bytes 12582916
  6.9 39.6 %copy-start.1 = (bf16[1,128,4096]{2,1,0:T(8,128)(2,1)S(1)}, bf16[1,128,4096]{2,1,0:T(8,128)(2,1)}, u32[]{:S(2)}) copy-start(bf16[1,128,4096]{2,1,0:T(8,128)(2,1)} %param.20) | copy-start | bytes 3145732
  6.9 39.6 %copy-start.6 = (f32[4096]{0:T(1024)S(1)}, f32[4096]{0:T(1024)}, u32[]{:S(2)}) copy-start(f32[4096]{0:T(1024)} %param.22) | copy-start | bytes 49156
  46.5 28.6 %copy-start.11 = (f32[8,8,128]{2,1,0:T(8,128)}, f32[8,8,128]{2,1,0:T(8,128)S(1)}, u32[]{:S(2)}) copy-start(f32[8,8,128]{2,1,0:T(8,128)S(1)} %get-tuple-element.11.packed_ref) | copy-start | bytes 98308
  75.1 1.0 copy-start.9
  76.1 1.0 copy-start.10
